TPU v7x, 32 devices: a whole 2x2x4 slice. The times are simulated.
32 devices in a mesh: rep: 2 (over x), fs: 8 (over z, y), tp: 2 (over core).
Axes of the slice: x: 2, y: 2, z: 4, core: 2. Of those that a mesh axis runs over, the one named last changes fastest.
Arguments:
- tokens: bfloat16 [6144, 2048], P(('rep', 'fs'), 'tp'), may hold values from -6 to 6
- mixing_norm_gain: float32 [2048], replicated, may hold values from 0.1 to 1.9
- recurrent_input_weight: float32 [2048, 3072], P('fs', 'tp'), may hold values from -0.125 to 0.125
- recurrent_input_scale: float32 [3072], P('tp'), may hold values from 0.5 to 2
- convolution_kernel_taps: float32 [4, 3072], P(None, 'tp'), may hold values from -3 to 3
- recurrence_gate_weight_blocks: bfloat16 [24, 128, 128], P('tp'), may hold values from -0.5 to 0.5
- input_gate_weight_blocks: bfloat16 [24, 128, 128], P('tp'), may hold values from -0.5 to 0.5
- channel_decay_parameter: float32 [3072], P('tp'), may hold values from 3 to 9
- token_extra_log_decay: float32 [6144], P(('rep', 'fs')), may hold values from -0.7 to 0
- mixing_output_weight: float32 [3072, 2048], P('tp', 'fs'), may hold values from -0.109375 to 0.109375
- mixing_output_scale: float32 [2048], P('fs'), may hold values from 0.5 to 2
- feedforward_norm_gain: float32 [2048], replicated, may hold values from 0.1 to 1.9
- feedforward_gate_weight: float32 [2048, 5120], P('fs', 'tp'), may hold values from -0.125 to 0.125
- feedforward_gate_scale: float32 [5120], P('tp'), may hold values from 0.5 to 2
- feedforward_up_weight: float32 [2048, 5120], P('fs', 'tp'), may hold values from -0.125 to 0.125
- feedforward_up_scale: float32 [5120], P('tp'), may hold values from 0.5 to 2
- feedforward_down_weight: float32 [5120, 2048], P('tp', 'fs'), may hold values from -0.078125 to 0.078125
- feedforward_down_scale: float32 [2048], P('fs'), may hold values from 0.5 to 2
Outputs:
- layer_out: bfloat16 [6144, 2048], P(('rep', 'fs'), 'tp')
All inputs are finite; a program needn't handle non-finite values.
Results may differ from a plain program's by a relative error of at most 0.02.
Values may be sent and summed in bfloat16 or wider, within the bound.
A program may use at most 128 MiB of HBM per device.

v0:
```python
import jax
import jax.numpy as jnp
from jax import lax
from jax.sharding import PartitionSpec as P

EPS = 1e-06
DECAY_FACTOR = 8.0


def row_norm(rows, gain_vec):
    values = rows.astype(jnp.float32)
    inverse = lax.rsqrt(jnp.mean(values * values, axis=-1, keepdims=True) + EPS)
    return (values * inverse * gain_vec).astype(jnp.bfloat16)


def gather_normed(rows, gain_vec):
    whole_rows = lax.all_gather(rows, "tp", axis=1, tiled=True)
    return row_norm(whole_rows, gain_vec)


def share_sums(terms):
    return lax.psum_scatter(
        terms.astype(jnp.bfloat16), "tp", scatter_dimension=1, tiled=True
    ).astype(jnp.float32)


def combine_pairs(earlier, later):
    decay_one, value_one = earlier
    decay_two, value_two = later
    return (decay_one * decay_two, decay_two * value_one + value_two)


def add_one(left_rows, weight_piece):
    return jnp.dot(left_rows, weight_piece, preferred_element_type=jnp.float32)


def place_columns(left_rows, total_now, pieces, start_row):
    weight_piece, scale_piece = pieces
    product = jnp.dot(left_rows, weight_piece, preferred_element_type=jnp.float32) * scale_piece
    return lax.dynamic_update_slice_in_dim(total_now, product, start_row, 1)


def body(
    tokens,
    mixing_norm_gain,
    recurrent_input_weight,
    recurrent_input_scale,
    convolution_kernel_taps,
    recurrence_gate_weight_blocks,
    input_gate_weight_blocks,
    channel_decay_parameter,
    token_extra_log_decay,
    mixing_output_weight,
    mixing_output_scale,
    feedforward_norm_gain,
    feedforward_gate_weight,
    feedforward_gate_scale,
    feedforward_up_weight,
    feedforward_up_scale,
    feedforward_down_weight,
    feedforward_down_scale,
):
    normed = gather_normed(tokens, mixing_norm_gain)
    seq_rows = normed.shape[0]
    model_width = normed.shape[1]
    width_dev = recurrent_input_weight.shape[1]
    rec_sum = add_one(
        normed,
        lax.all_gather(recurrent_input_weight.astype(jnp.bfloat16), "fs", axis=0, tiled=True),
    )
    rec_input = (rec_sum * recurrent_input_scale).astype(jnp.bfloat16)
    rec_f32 = rec_input.astype(jnp.float32)
    tap_count = convolution_kernel_taps.shape[0]
    padded = jnp.pad(rec_f32, ((tap_count - 1, 0), (0, 0)))
    conv_out = jnp.zeros((seq_rows, width_dev), jnp.float32)
    for tap_index in range(tap_count):
        conv_out = (
            conv_out + convolution_kernel_taps[tap_index] * padded[tap_index : tap_index + seq_rows]
        )
    block_count = recurrence_gate_weight_blocks.shape[0]
    block_size = recurrence_gate_weight_blocks.shape[1]
    blocks = conv_out.astype(jnp.bfloat16).reshape(seq_rows, block_count, block_size)
    recurrence_gate_values = jax.nn.sigmoid(
        jnp.einsum(
            "lni,nij->lnj",
            blocks,
            recurrence_gate_weight_blocks,
            preferred_element_type=jnp.float32,
        ).reshape(seq_rows, width_dev)
    )
    input_gate = jax.nn.sigmoid(
        jnp.einsum(
            "lni,nij->lnj", blocks, input_gate_weight_blocks, preferred_element_type=jnp.float32
        ).reshape(seq_rows, width_dev)
    )
    decay_logarithm = (
        -DECAY_FACTOR * recurrence_gate_values * jax.nn.softplus(-channel_decay_parameter)
        + token_extra_log_decay[:, None]
    )
    decay = jnp.exp(decay_logarithm)
    drive = jnp.sqrt(-jnp.expm1(2.0 * decay_logarithm)) * input_gate * conv_out
    _, state = lax.associative_scan(combine_pairs, (decay, drive), axis=0)
    state_low = state.astype(jnp.bfloat16)
    mix_terms = place_columns(
        state_low,
        jnp.zeros((seq_rows, model_width), jnp.float32),
        (
            lax.all_gather(mixing_output_weight.astype(jnp.bfloat16), "fs", axis=1, tiled=True),
            lax.all_gather(
                mixing_output_scale.reshape(1, -1).astype(jnp.bfloat16), "fs", axis=1, tiled=True
            ).astype(jnp.float32),
        ),
        jnp.int32(0),
    )
    mixed = (tokens.astype(jnp.float32) + share_sums(mix_terms)).astype(jnp.bfloat16)
    normed_ffn = gather_normed(mixed, feedforward_norm_gain)
    gate_sum = add_one(
        normed_ffn,
        lax.all_gather(feedforward_gate_weight.astype(jnp.bfloat16), "fs", axis=0, tiled=True),
    )
    up_sum = add_one(
        normed_ffn,
        lax.all_gather(feedforward_up_weight.astype(jnp.bfloat16), "fs", axis=0, tiled=True),
    )
    hidden = (
        jax.nn.silu(gate_sum * feedforward_gate_scale) * (up_sum * feedforward_up_scale)
    ).astype(jnp.bfloat16)
    down_terms = place_columns(
        hidden,
        jnp.zeros((seq_rows, model_width), jnp.float32),
        (
            lax.all_gather(feedforward_down_weight.astype(jnp.bfloat16), "fs", axis=1, tiled=True),
            lax.all_gather(
                feedforward_down_scale.reshape(1, -1).astype(jnp.bfloat16), "fs", axis=1, tiled=True
            ).astype(jnp.float32),
        ),
        jnp.int32(0),
    )
    return (mixed.astype(jnp.float32) + share_sums(down_terms)).astype(jnp.bfloat16)


def solution(mesh):
    placed = (
        P(("rep", "fs"), "tp"),
        P(),
        P("fs", "tp"),
        P("tp"),
        P(None, "tp"),
        P("tp", None, None),
        P("tp", None, None),
        P("tp"),
        P(("rep", "fs")),
        P("tp", "fs"),
        P("fs"),
        P(),
        P("fs", "tp"),
        P("tp"),
        P("fs", "tp"),
        P("tp"),
        P("tp", "fs"),
        P("fs"),
    )
    return jax.shard_map(
        body, mesh=mesh, in_specs=placed, out_specs=P(("rep", "fs"), "tp"), check_vma=False
    )
```

profile of v0, /device:TPU:0, one launch (start us, length us, event | category | flops | bytes accessed | tf_op | source)
XLA Modules:
  0.0 784.1 jit_solution(13299143010067147832)
XLA Ops:
  7.3 2.4 convert_element_type.85
  9.8 1.0 convert_element_type.90
  11.0 22.3 %all-gather.2 = bf16[8,1,256]{2,1,0:T(2,128)(2,1)S(1)} all-gather(bf16[1,1,256]{2,1,0:T(2,128)(2,1)S(1)} %reshape.53), channel_id=2, replica_groups=mesh['rep'=2,'fs'=8,'tp'=2] {'fs'}, dimensions={0}, use_global_device_ids=true | all-gather | bytes 4608 | tf_op jit(solution)/shard_map/all_gather | solution.py:109
  33.9 1.9 fusion.2
  35.8 87.7 %all-gather.14.cloned.1.call-done = bf16[2048,1536]{1,0:T(8,128)(2,1)} async-done(((bf16[256,1536]{1,0:T(8,128)(2,1)}), bf16[2048,1536]{1,0:T(8,128)(2,1)}) %all-gather.14.cloned.1.call-update) | async-done | bytes 6291472 | tf_op jit(solution)/shard_map/all_gather | solution.py:69
  123.5 5.3 fusion.9
  128.8 2.5 fusion.29
  131.3 1.4 copy.32
  132.7 2.1 add_divide_fusion.1
  134.9 2.1 copy.35
  136.9 2.1 add_divide_fusion
  139.1 2.0 copy.38
  141.0 6.5 fusion.11
  147.5 2.9 slice.221
  150.4 2.9 slice.222
  153.3 5.5 slice.220
  158.8 5.5 slice.224
  164.3 4.1 fusion.30
  168.4 3.3 slice.227
  171.8 3.3 slice.228
  175.0 3.3 slice.226
  178.4 3.3 slice.230
  181.7 2.6 fusion.31
  185.9 1.7 slice.232
  187.6 1.7 slice.236
  189.3 2.0 fusion.32
  192.7 1.7 slice.238
  194.4 1.6 slice.242
  196.0 1.8 fusion.33
  199.1 1.6 slice.244
  200.7 1.6 slice.248
  202.2 1.7 fusion.34
  205.2 1.5 slice.250
  206.7 1.5 slice.254
  208.2 1.5 fusion.35
  211.0 1.4 slice.256
  212.4 1.4 slice.260
  218.0 1.6 slice.243
  220.8 1.0 slice.237
  223.1 1.8 slice.231
  226.4 3.4 slice.225
  229.7 3.3 slice.276
  233.0 1.4 slice.280
  234.5 3.1 slice.278
  237.6 5.6 slice.219
  248.2 1.2 add.203
  249.4 9.0 %pad.69 = f32[384,1536]{1,0:T(8,128)} pad(f32[192,1536]{1,0:T(8,128)} %add.203, f32[]{:T(128)} %constant.7.clone.1), padding=1_0_1x0_0_0 | pad | bytes 3538948 | tf_op jit(solution)/shard_map/pad | solution.py:102
  258.4 2.0 fusion.15
  260.5 5.0 pad.68
  265.5 8.1 %multiply_convert_fusion.1 = bf16[384,2048]{1,0:T(8,128)(2,1)} fusion(bf16[1536,2048]{1,0:T(8,128)(2,1)} %all-gather.16.cloned.1.call-done, f32[2048]{0:T(1024)S(1)} %bitcast.22, f32[384,1536]{1,0:T(8,128)} %pad.68, f32[384,1536]{1,0:T(8,128)} %pad.69), kind=kOutput, calls=%fused_computation.15 | convolution fusion | flops 2418671616 | bytes 12591104 | tf_op jit(solution)/shard_map/dot_general | solution.py:39
  273.7 7.3 reduce-scatter.3.cloned.1.call-done
  281.0 2.3 add_convert_fusion.2
  283.4 3.1 convert_element_type.99
  286.6 1.2 convert_element_type.100
  287.9 2.9 convert_element_type.102
  290.9 20.9 %all-gather.3 = bf16[8,1,256]{2,1,0:T(2,128)(2,1)S(1)} all-gather(bf16[1,1,256]{2,1,0:T(2,128)(2,1)S(1)} %reshape.55), channel_id=3, replica_groups=mesh['rep'=2,'fs'=8,'tp'=2] {'fs'}, dimensions={0}, use_global_device_ids=true | all-gather | bytes 4608 | tf_op jit(solution)/shard_map/all_gather | solution.py:133
  311.9 1.8 fusion.5
  313.7 134.7 %all-gather.20.cloned.1.call-done = bf16[2048,2560]{1,0:T(8,128)(2,1)} async-done(((bf16[256,2560]{1,0:T(8,128)(2,1)}), bf16[2048,2560]{1,0:T(8,128)(2,1)}) %all-gather.20.cloned.1.call-update) | async-done | bytes 10485776 | tf_op jit(solution)/shard_map/all_gather | solution.py:119
  448.4 10.6 %convolution_multiply_fusion.1 = f32[384,2560]{1,0:T(8,128)} fusion(bf16[2048,2560]{1,0:T(8,128)(2,1)} %all-gather.20.cloned.1.call-done, f32[2560]{0:T(1024)S(1)} %copy-done.30, bf16[384,2048]{1,0:T(8,128)(2,1)} %all-gather.18.cloned.1.call-done, f32[2048]{0:T(1024)S(1)} %copy-done.34, f32[384]{0:T(512)S(1)} %add_rsqrt_fusion), kind=kOutput, calls=%fused_computation.2 | convolution fusion | flops 4030660608 | bytes 16010752 | tf_op jit(solution)/shard_map/dot_general | solution.py:34
  459.0 140.3 %all-gather.22.cloned.1.call-done = bf16[2048,2560]{1,0:T(8,128)(2,1)} async-done(((bf16[256,2560]{1,0:T(8,128)(2,1)}), bf16[2048,2560]{1,0:T(8,128)(2,1)}) %all-gather.22.cloned.1.call-update) | async-done | bytes 10485776 | tf_op jit(solution)/shard_map/all_gather | solution.py:123
  599.3 150.8 %all-gather.24.cloned.1.call-done = bf16[2560,2048]{1,0:T(8,128)(2,1)} async-done(((bf16[2560,256]{1,0:T(8,128)(2,1)}), bf16[2560,2048]{1,0:T(8,128)(2,1)}) %all-gather.24.cloned.1.call-update) | async-done | bytes 10485776 | tf_op jit(solution)/shard_map/all_gather | solution.py:132
  750.1 17.9 %multiply_convert_fusion = bf16[384,2048]{1,0:T(8,128)(2,1)} fusion(bf16[2560,2048]{1,0:T(8,128)(2,1)} %all-gather.24.cloned.1.call-done, f32[2048]{0:T(1024)S(1)} %bitcast.23, bf16[2048,2560]{1,0:T(8,128)(2,1)} %all-gather.22.cloned.1.call-done, f32[384,2560]{1,0:T(8,128)} %convolution_multiply_fusion.1, f32[2560]{0:T(1024)S(1)} %copy-done.31, ...), kind=kOutput, calls=%fused_computation.14 | convolution fusion | flops 8064663552 | bytes 28077568 | tf_op jit(solution)/shard_map/dot_general | solution.py:39
  768.0 7.3 reduce-scatter.5.cloned.1.call-done
  775.3 2.3 add_convert_fusion.1
  (163 shorter events, 21.7 us)
Async XLA Ops:
  6.5 126.2 %copy-start = (bf16[12,128,128]{2,1,0:T(8,128)(2,1)S(1)}, bf16[12,128,128]{2,1,0:T(8,128)(2,1)}, u32[]{:S(2)}) copy-start(bf16[12,128,128]{2,1,0:T(8,128)(2,1)} %param.23) | copy-start | bytes 1179652
  6.5 3.3 copy-start.7
  6.5 27.4 %all-gather.12.cloned.1.call-start = ((), (), s32[]{:S(2)}) async-start(), calls=%async_computation.2 | async-start | bytes 2359296 | tf_op jit(solution)/shard_map/all_gather | solution.py:17
  7.3 116.3 %all-gather.14.cloned.1.call-start = ((), (), s32[]{:S(2)}) async-start(), calls=%async_computation.3 | async-start | bytes 7077888 | tf_op jit(solution)/shard_map/all_gather | solution.py:69
  9.7 1.1 copy-start.21
  9.7 1.2 copy-start.26
  9.7 1.3 copy-start.35
  9.7 113.8 %copy-start.32 = (f32[2048]{0:T(1024)S(1)}, f32[2048]{0:T(1024)}, u32[]{:S(2)}) copy-start(f32[2048]{0:T(1024)} %param.19) | copy-start | bytes 24580
  9.8 113.8 %copy-start.33 = (f32[1536]{0:T(1024)S(1)}, f32[1536]{0:T(1024)}, u32[]{:S(2)}) copy-start(f32[1536]{0:T(1024)} %param.21) | copy-start | bytes 18436
  9.8 255.7 %all-gather.16.cloned.1.call-start = ((), (), s32[]{:S(2)}) async-start(), calls=%async_computation.4 | async-start | bytes 7077888 | tf_op jit(solution)/shard_map/all_gather | solution.py:108
  10.8 270.2 %reduce-scatter.3.cloned.1.call-start = ((), (), s32[]{:S(2)}) async-start(), calls=%async_computation.5 | async-start | bytes 2359296 | tf_op jit(solution)/shard_map/reduce_scatter | solution.py:22
  134.9 2.1 copy-start.29
  139.0 2.0 copy-start.28
  234.4 9.4 %copy-start.14 = (f32[3,1536]{1,0:T(4,128)S(1)}, f32[3,1536]{1,0:T(4,128)}, u32[]{:S(2)}) copy-start(f32[3,1536]{1,0:T(4,128)} %slice.257) | copy-start | bytes 55300
  234.4 9.4 %copy-start.15 = (f32[3,1536]{1,0:T(4,128)S(1)}, f32[3,1536]{1,0:T(4,128)}, u32[]{:S(2)}) copy-start(f32[3,1536]{1,0:T(4,128)} %slice.258) | copy-start | bytes 55300
  234.4 9.4 %copy-start.16 = (f32[3,1536]{1,0:T(4,128)S(1)}, f32[3,1536]{1,0:T(4,128)}, u32[]{:S(2)}) copy-start(f32[3,1536]{1,0:T(4,128)} %slice.256) | copy-start | bytes 55300
  234.4 9.4 %copy-start.17 = (f32[3,1536]{1,0:T(4,128)S(1)}, f32[3,1536]{1,0:T(4,128)}, u32[]{:S(2)}) copy-start(f32[3,1536]{1,0:T(4,128)} %slice.260) | copy-start | bytes 55300
  234.4 9.5 %copy-start.18 = (f32[2,1536]{1,0:T(2,128)S(1)}, f32[2,1536]{1,0:T(2,128)}, u32[]{:S(2)}) copy-start(f32[2,1536]{1,0:T(2,128)} %slice.266) | copy-start | bytes 36868
  234.5 9.6 %copy-start.23 = (f32[1,1536]{1,0:T(1,128)S(1)}, f32[1,1536]{1,0:T(1,128)}, u32[]{:S(2)}) copy-start(f32[1,1536]{1,0:T(1,128)} %slice.285) | copy-start | bytes 18436
  234.5 9.6 %copy-start.13 = (f32[5,1536]{1,0:T(8,128)S(1)}, f32[5,1536]{1,0:T(8,128)}, u32[]{:S(2)}) copy-start(f32[5,1536]{1,0:T(8,128)} %slice.268) | copy-start | bytes 92164
  234.5 9.6 %copy-start.22 = (f32[1,1536]{1,0:T(1,128)S(1)}, f32[1,1536]{1,0:T(1,128)}, u32[]{:S(2)}) copy-start(f32[1,1536]{1,0:T(1,128)} %slice.284) | copy-start | bytes 18436
  237.6 6.7 copy-start.11
  237.6 6.7 copy-start.12
  243.8 2.3 copy-start.24
  244.3 2.1 copy-start.9
  244.3 2.1 copy-start.10
  246.1 0.7 copy-start.20
  246.4 1.1 copy-start.5
  246.4 1.2 copy-start.6
  246.9 0.8 copy-start.19
  258.4 2.0 copy-start.25
  260.5 5.0 copy-start.27
  265.5 15.5 %copy-start.3 = (bf16[384,1024]{1,0:T(8,128)(2,1)S(1)}, bf16[384,1024]{1,0:T(8,128)(2,1)}, u32[]{:S(2)}) copy-start(bf16[384,1024]{1,0:T(8,128)(2,1)} %param.18) | copy-start | bytes 2359300
  273.7 38.2 %all-gather.18.cloned.1.call-start = ((), (), s32[]{:S(2)}) async-start(), calls=%async_computation.6 | async-start | bytes 2359296 | tf_op jit(solution)/shard_map/all_gather | solution.py:17
  283.4 3.2 copy-start.4
  283.4 165.0 %all-gather.20.cloned.1.call-start = ((), (), s32[]{:S(2)}) async-start(), calls=%async_computation.7 | async-start | bytes 11796480 | tf_op jit(solution)/shard_map/all_gather | solution.py:119
  286.5 312.7 %all-gather.22.cloned.1.call-start = ((), (), s32[]{:S(2)}) async-start(), calls=%async_computation.8 | async-start | bytes 11796480 | tf_op jit(solution)/shard_map/all_gather | solution.py:123
  287.8 3.1 copy-start.36
  287.8 462.2 %all-gather.24.cloned.1.call-start = ((), (), s32[]{:S(2)}) async-start(), calls=%async_computation.9 | async-start | bytes 11796480 | tf_op jit(solution)/shard_map/all_gather | solution.py:132
  290.8 157.5 %copy-start.30 = (f32[2560]{0:T(1024)S(1)}, f32[2560]{0:T(1024)}, u32[]{:S(2)}) copy-start(f32[2560]{0:T(1024)} %param.31) | copy-start | bytes 30724
  290.8 157.5 %copy-start.34 = (f32[2048]{0:T(1024)S(1)}, f32[2048]{0:T(1024)}, u32[]{:S(2)}) copy-start(f32[2048]{0:T(1024)} %param.29) | copy-start | bytes 24580
  290.9 484.4 %reduce-scatter.5.cloned.1.call-start = ((), (), s32[]{:S(2)}) async-start(), calls=%async_computation.10 | async-start | bytes 2359296 | tf_op jit(solution)/shard_map/reduce_scatter | solution.py:22
  313.7 436.4 %copy-start.8 = (bf16[384,2048]{1,0:T(8,128)(2,1)S(1)}, bf16[384,2048]{1,0:T(8,128)(2,1)}, u32[]{:S(2)}) copy-start(bf16[384,2048]{1,0:T(8,128)(2,1)} %all-gather.18.cloned.1.call-done) | copy-start | bytes 4718596
  313.7 436.4 %copy-start.31 = (f32[2560]{0:T(1024)S(1)}, f32[2560]{0:T(1024)}, u32[]{:S(2)}) copy-start(f32[2560]{0:T(1024)} %param.33) | copy-start | bytes 30724
  750.1 25.2 %copy-start.2 = (bf16[384,1024]{1,0:T(8,128)(2,1)S(1)}, bf16[384,1024]{1,0:T(8,128)(2,1)}, u32[]{:S(2)}) copy-start(bf16[384,1024]{1,0:T(8,128)(2,1)} %add_convert_fusion.2) | copy-start | bytes 2359300
  750.1 27.5 %copy-start.1 = (bf16[12,128,128]{2,1,0:T(8,128)(2,1)S(1)}, bf16[12,128,128]{2,1,0:T(8,128)(2,1)}, u32[]{:S(2)}) copy-start(bf16[12,128,128]{2,1,0:T(8,128)(2,1)} %param.23) | copy-start | bytes 1179652
Sparse Core Ops, SparseCore 0:
  8.9 12.5 all-gather.11
  23.6 99.8 all-gather.13
  125.6 97.6 all-gather.15
  273.8 7.1 reduce-scatter.2
  283.5 11.0 all-gather.17
  296.6 151.6 all-gather.19
  450.6 148.6 all-gather.21
  601.3 148.6 all-gather.23
  768.1 7.0 reduce-scatter.4
where the time goes:
time: 786 us; the launch traced here: 784 us
  waiting for transfers between devices  529 us (67%)
  local copies, waits for them, and re-layouts  104 us (13%)
  other arithmetic  48 us (6%)
  matrix products  46.2 us (6%)
  blocking collectives  43.2 us (5%)
  between operations  13.9 us (2%)
    all_gather x1, waiting for transfers between devices, body(): lax.all_gather(feedforward_down_weight.astype(jnp.bfloat16), 'fs', axis=1...  151 us
    all_gather x1, waiting for transfers between devices, body(): lax.all_gather(feedforward_up_weight.astype(jnp.bfloat16), 'fs', axis=0,...  140 us
    all_gather x1, waiting for transfers between devices, body(): lax.all_gather(feedforward_gate_weight.astype(jnp.bfloat16), 'fs', axis=0...  135 us
    all_gather x1, waiting for transfers between devices, body(): lax.all_gather(recurrent_input_weight.astype(jnp.bfloat16), 'fs', axis=0,...  87.7 us
    slice x49, local copies, waits for them, and re-layouts, body(): _, state = lax.associative_scan(combine_pairs, (decay, drive), axis=0)  82.4 us
    dot_general x2, matrix products, place_columns(): jnp.dot(left_rows, weight_piece, preferred_element_type=jnp.float32)  26.1 us
    all_gather x1, blocking collectives, body(): lax.all_gather(mixing_output_scale.reshape(1, -1).astype(jnp.bfloat16), '...  22.3 us
    all_gather x1, blocking collectives, body(): lax.all_gather(feedforward_down_scale.reshape(1, -1).astype(jnp.bfloat16)...  20.9 us
  transfers between devices with their start and end apart: 9, of which 6 were waited for; matrix products, arithmetic and copies ran while one was open for 21% of the time, Pallas kernels for 0%

commit v1 on v0

--- a/solution.py
+++ b/solution.py
@@ -5,6 +5,13 @@
 
 EPS = 1e-06
 DECAY_FACTOR = 8.0
+
+
+def swapped_in(x, mesh_axis, along):
+    devices = lax.axis_size(mesh_axis)
+    blocks = jnp.stack([x for _ in range(devices)])
+    blocks = lax.all_to_all(blocks, mesh_axis, split_axis=0, concat_axis=0)
+    return jnp.concatenate(blocks, axis=along)
 
 
 def row_norm(rows, gain_vec):
@@ -64,10 +71,7 @@
     seq_rows = normed.shape[0]
     model_width = normed.shape[1]
     width_dev = recurrent_input_weight.shape[1]
-    rec_sum = add_one(
-        normed,
-        lax.all_gather(recurrent_input_weight.astype(jnp.bfloat16), "fs", axis=0, tiled=True),
-    )
+    rec_sum = add_one(normed, swapped_in(recurrent_input_weight.astype(jnp.bfloat16), "fs", 0))
     rec_input = (rec_sum * recurrent_input_scale).astype(jnp.bfloat16)
     rec_f32 = rec_input.astype(jnp.float32)
     tap_count = convolution_kernel_taps.shape[0]

time: 786 us -> 905 us (1.15)
  blocking collectives: 43.2 us -> 161 us
    all_gather x1, blocking collectives: 22.3 us -> 140 us  [body(): lax.all_gather(mixing_output_scale.reshape(1, -1).astype(jnp.bfloat16), '...]
    all_gather x1 -> x0, waiting for transfers between devices: 87.7 us -> none  [body(): lax.all_gather(recurrent_input_weight.astype(jnp.bfloat16), 'fs', axis=0,...]
    all_to_all x0 -> x1, waiting for transfers between devices: none -> 67.2 us  [swapped_in(): blocks = lax.all_to_all(blocks, mesh_axis, split_axis=0, concat_axis=0)]
    reduce_scatter x2, waiting for transfers between devices: 14.6 us -> 26 us  [share_sums(): lax.psum_scatter(terms.astype(jnp.bfloat16), 'tp', scatter_dimension=1, t...]
  transfers between devices with their start and end apart: 9 -> 9, of which waited for: 6 -> 6; matrix products, arithmetic and copies ran while one was open for 21% -> 18% of each run, Pallas kernels for 0% -> 0%
where the time goes in v1:
time: 905 us; the launch traced here: 903 us
  waiting for transfers between devices  520 us (57%)
  blocking collectives  161 us (18%)
  local copies, waits for them, and re-layouts  107 us (12%)
  other arithmetic  47 us (5%)
  matrix products  46.1 us (5%)
  between operations  14.2 us (2%)
    all_gather x1, waiting for transfers between devices, body(): lax.all_gather(feedforward_down_weight.astype(jnp.bfloat16), 'fs', axis=1...  151 us
    all_gather x1, blocking collectives, body(): lax.all_gather(mixing_output_scale.reshape(1, -1).astype(jnp.bfloat16), '...  140 us
    all_gather x1, waiting for transfers between devices, body(): lax.all_gather(feedforward_up_weight.astype(jnp.bfloat16), 'fs', axis=0,...  140 us
    all_gather x1, waiting for transfers between devices, body(): lax.all_gather(feedforward_gate_weight.astype(jnp.bfloat16), 'fs', axis=0...  135 us
    slice x49, local copies, waits for them, and re-layouts, body(): _, state = lax.associative_scan(combine_pairs, (decay, drive), axis=0)  82.4 us
    all_to_all x1, waiting for transfers between devices, swapped_in(): blocks = lax.all_to_all(blocks, mesh_axis, split_axis=0, concat_axis=0)  67.2 us
    dot_general x2, matrix products, place_columns(): jnp.dot(left_rows, weight_piece, preferred_element_type=jnp.float32)  26.1 us
    reduce_scatter x2, waiting for transfers between devices, share_sums(): lax.psum_scatter(terms.astype(jnp.bfloat16), 'tp', scatter_dimension=1, t...  26 us
  transfers between devices with their start and end apart: 9, of which 6 were waited for; matrix products, arithmetic and copies ran while one was open for 18% of the time, Pallas kernels for 0%

profile of v1, /device:TPU:0, one launch (start us, length us, event | category | flops | bytes accessed | tf_op | source)
XLA Modules:
  0.0 903.0 jit_solution(7860505882854231391)
XLA Ops:
  6.5 1.5 convert_element_type.85
  8.1 3.1 stack.2
  11.2 7.4 all-to-all-start
  20.6 140.4 %all-gather.2 = bf16[8,1,256]{2,1,0:T(2,128)(2,1)S(1)} all-gather(bf16[1,1,256]{2,1,0:T(2,128)(2,1)S(1)} %reshape.59), channel_id=2, replica_groups=mesh['rep'=2,'fs'=8,'tp'=2] {'fs'}, dimensions={0}, use_global_device_ids=true | all-gather | bytes 4608 | tf_op jit(solution)/shard_map/all_gather | solution.py:113
  161.8 1.8 fusion.2
  163.6 67.2 %all-to-all-done = bf16[8,256,1536]{2,1,0:T(8,128)(2,1)} async-done(((bf16[8,256,1536]{2,1,0:T(8,128)(2,1)}), bf16[8,256,1536]{2,1,0:T(8,128)(2,1)}, u32[]{:S(2)}, u32[]{:S(2)}) %all-to-all-start) | async-done | bytes 6291488 | tf_op jit(solution)/shard_map/all_to_all | solution.py:13
  230.8 5.3 fusion.9
  236.1 2.5 fusion.29
  238.6 1.4 copy.32
  240.0 2.1 add_divide_fusion.1
  242.1 2.1 copy.35
  244.1 2.1 add_divide_fusion
  246.2 2.0 copy.38
  248.2 6.5 fusion.11
  254.7 2.9 slice.221
  257.7 2.9 slice.222
  260.5 5.5 slice.220
  266.0 5.5 slice.224
  271.5 4.1 fusion.30
  275.6 3.3 slice.227
  278.9 3.3 slice.228
  282.2 3.3 slice.226
  285.5 3.3 slice.230
  288.8 2.6 fusion.31
  293.0 1.7 slice.232
  294.8 1.7 slice.236
  296.5 2.0 fusion.32
  299.9 1.7 slice.238
  301.6 1.6 slice.242
  303.2 1.8 fusion.33
  306.3 1.6 slice.244
  307.9 1.6 slice.248
  309.5 1.7 fusion.34
  312.4 1.5 slice.250
  313.9 1.5 slice.254
  315.4 1.5 fusion.35
  318.2 1.4 slice.256
  319.6 1.4 slice.260
  325.2 1.6 slice.243
  330.3 1.8 slice.231
  333.5 3.4 slice.225
  336.9 3.3 slice.276
  340.2 1.4 slice.280
  341.7 3.1 slice.278
  344.8 5.6 slice.219
  355.4 1.2 add.203
  356.6 9.0 %pad.69 = f32[384,1536]{1,0:T(8,128)} pad(f32[192,1536]{1,0:T(8,128)} %add.203, f32[]{:T(128)} %constant.7.clone.1), padding=1_0_1x0_0_0 | pad | bytes 3538948 | tf_op jit(solution)/shard_map/pad | solution.py:106
  365.6 2.0 fusion.15
  367.8 5.0 pad.68
  372.8 8.1 multiply_convert_fusion.1
  381.0 18.7 %reduce-scatter.3.cloned.1.call-done = bf16[384,1024]{1,0:T(8,128)(2,1)} async-done(((bf16[384,2048]{1,0:T(8,128)(2,1)}), bf16[384,1024]{1,0:T(8,128)(2,1)}) %reduce-scatter.3.cloned.1.call-update) | async-done | bytes 786448 | tf_op jit(solution)/shard_map/reduce_scatter | solution.py:29
  399.8 2.3 add_convert_fusion.2
  402.2 3.1 convert_element_type.99
  405.4 1.2 convert_element_type.100
  406.7 2.9 convert_element_type.102
  409.7 20.9 %all-gather.3 = bf16[8,1,256]{2,1,0:T(2,128)(2,1)S(1)} all-gather(bf16[1,1,256]{2,1,0:T(2,128)(2,1)S(1)} %reshape.61), channel_id=3, replica_groups=mesh['rep'=2,'fs'=8,'tp'=2] {'fs'}, dimensions={0}, use_global_device_ids=true | all-gather | bytes 4608 | tf_op jit(solution)/shard_map/all_gather | solution.py:137
  430.6 1.8 fusion.5
  432.5 134.6 %all-gather.17.cloned.1.call-done = bf16[2048,2560]{1,0:T(8,128)(2,1)} async-done(((bf16[256,2560]{1,0:T(8,128)(2,1)}), bf16[2048,2560]{1,0:T(8,128)(2,1)}) %all-gather.17.cloned.1.call-update) | async-done | bytes 10485776 | tf_op jit(solution)/shard_map/all_gather | solution.py:123
  567.1 10.6 %convolution_multiply_fusion.1 = f32[384,2560]{1,0:T(8,128)} fusion(bf16[2048,2560]{1,0:T(8,128)(2,1)} %all-gather.17.cloned.1.call-done, f32[2560]{0:T(1024)S(1)} %copy-done.30, bf16[384,2048]{1,0:T(8,128)(2,1)} %all-gather.15.cloned.1.call-done, f32[2048]{0:T(1024)S(1)} %copy-done.34, f32[384]{0:T(512)S(1)} %add_rsqrt_fusion), kind=kOutput, calls=%fused_computation.2 | convolution fusion | flops 4030660608 | bytes 16010752 | tf_op jit(solution)/shard_map/dot_general | solution.py:41
  577.7 140.2 %all-gather.19.cloned.1.call-done = bf16[2048,2560]{1,0:T(8,128)(2,1)} async-done(((bf16[256,2560]{1,0:T(8,128)(2,1)}), bf16[2048,2560]{1,0:T(8,128)(2,1)}) %all-gather.19.cloned.1.call-update) | async-done | bytes 10485776 | tf_op jit(solution)/shard_map/all_gather | solution.py:127
  717.9 150.8 %all-gather.21.cloned.1.call-done = bf16[2560,2048]{1,0:T(8,128)(2,1)} async-done(((bf16[2560,256]{1,0:T(8,128)(2,1)}), bf16[2560,2048]{1,0:T(8,128)(2,1)}) %all-gather.21.cloned.1.call-update) | async-done | bytes 10485776 | tf_op jit(solution)/shard_map/all_gather | solution.py:136
  868.6 17.9 %multiply_convert_fusion = bf16[384,2048]{1,0:T(8,128)(2,1)} fusion(bf16[2560,2048]{1,0:T(8,128)(2,1)} %all-gather.21.cloned.1.call-done, f32[2048]{0:T(1024)S(1)} %bitcast.24, bf16[2048,2560]{1,0:T(8,128)(2,1)} %all-gather.19.cloned.1.call-done, f32[384,2560]{1,0:T(8,128)} %convolution_multiply_fusion.1, f32[2560]{0:T(1024)S(1)} %copy-done.31, ...), kind=kOutput, calls=%fused_computation.14 | convolution fusion | flops 8064663552 | bytes 28077568 | tf_op jit(solution)/shard_map/dot_general | solution.py:46
  886.6 7.3 reduce-scatter.5.cloned.1.call-done
  893.9 2.3 add_convert_fusion.1
  (163 shorter events, 23.7 us)
Async XLA Ops:
  6.5 233.4 %copy-start = (bf16[12,128,128]{2,1,0:T(8,128)(2,1)S(1)}, bf16[12,128,128]{2,1,0:T(8,128)(2,1)}, u32[]{:S(2)}) copy-start(bf16[12,128,128]{2,1,0:T(8,128)(2,1)} %param.23) | copy-start | bytes 1179652
  11.2 8.3 copy-start.7
  11.2 219.5 %all-to-all-start = ((bf16[8,256,1536]{2,1,0:T(8,128)(2,1)}), bf16[8,256,1536]{2,1,0:T(8,128)(2,1)}, u32[]{:S(2)}, u32[]{:S(2)}) async-start(bf16[8,256,1536]{2,1,0:T(8,128)(2,1)} %stack.2), calls=%async_computation | async-start | bytes 12582912 | tf_op jit(solution)/shard_map/all_to_all | solution.py:13
  18.7 1.9 copy-start.35
  18.7 143.0 %copy-start.21 = (f32[4,1536]{1,0:T(4,128)S(1)}, f32[4,1536]{1,0:T(4,128)}, u32[]{:S(2)}) copy-start(f32[4,1536]{1,0:T(4,128)} %param.22) | copy-start | bytes 73732
  18.7 143.0 %copy-start.26 = (f32[1536]{0:T(1024)S(1)}, f32[1536]{0:T(1024)}, u32[]{:S(2)}) copy-start(f32[1536]{0:T(1024)} %param.25) | copy-start | bytes 18436
  18.7 143.1 %all-gather.11.cloned.1.call-start = ((), (), s32[]{:S(2)}) async-start(), calls=%async_computation.3 | async-start | bytes 2359296 | tf_op jit(solution)/shard_map/all_gather | solution.py:24
  19.4 211.3 %copy-start.32 = (f32[2048]{0:T(1024)S(1)}, f32[2048]{0:T(1024)}, u32[]{:S(2)}) copy-start(f32[2048]{0:T(1024)} %param.19) | copy-start | bytes 24580
  19.4 211.3 %copy-start.33 = (f32[1536]{0:T(1024)S(1)}, f32[1536]{0:T(1024)}, u32[]{:S(2)}) copy-start(f32[1536]{0:T(1024)} %param.21) | copy-start | bytes 18436
  19.4 353.3 %all-gather.13.cloned.1.call-start = ((), (), s32[]{:S(2)}) async-start(), calls=%async_computation.4 | async-start | bytes 7077888 | tf_op jit(solution)/shard_map/all_gather | solution.py:112
  20.5 379.3 %reduce-scatter.3.cloned.1.call-start = ((), (), s32[]{:S(2)}) async-start(), calls=%async_computation.5 | async-start | bytes 2359296 | tf_op jit(solution)/shard_map/reduce_scatter | solution.py:29
  242.1 2.1 copy-start.29
  246.2 2.0 copy-start.28
  341.6 9.4 %copy-start.14 = (f32[3,1536]{1,0:T(4,128)S(1)}, f32[3,1536]{1,0:T(4,128)}, u32[]{:S(2)}) copy-start(f32[3,1536]{1,0:T(4,128)} %slice.257) | copy-start | bytes 55300
  341.6 9.4 %copy-start.15 = (f32[3,1536]{1,0:T(4,128)S(1)}, f32[3,1536]{1,0:T(4,128)}, u32[]{:S(2)}) copy-start(f32[3,1536]{1,0:T(4,128)} %slice.258) | copy-start | bytes 55300
  341.6 9.4 %copy-start.16 = (f32[3,1536]{1,0:T(4,128)S(1)}, f32[3,1536]{1,0:T(4,128)}, u32[]{:S(2)}) copy-start(f32[3,1536]{1,0:T(4,128)} %slice.256) | copy-start | bytes 55300
  341.6 9.4 %copy-start.17 = (f32[3,1536]{1,0:T(4,128)S(1)}, f32[3,1536]{1,0:T(4,128)}, u32[]{:S(2)}) copy-start(f32[3,1536]{1,0:T(4,128)} %slice.260) | copy-start | bytes 55300
  341.6 9.5 %copy-start.18 = (f32[2,1536]{1,0:T(2,128)S(1)}, f32[2,1536]{1,0:T(2,128)}, u32[]{:S(2)}) copy-start(f32[2,1536]{1,0:T(2,128)} %slice.266) | copy-start | bytes 36868
  341.7 9.6 %copy-start.23 = (f32[1,1536]{1,0:T(1,128)S(1)}, f32[1,1536]{1,0:T(1,128)}, u32[]{:S(2)}) copy-start(f32[1,1536]{1,0:T(1,128)} %slice.285) | copy-start | bytes 18436
  341.7 9.6 %copy-start.13 = (f32[5,1536]{1,0:T(8,128)S(1)}, f32[5,1536]{1,0:T(8,128)}, u32[]{:S(2)}) copy-start(f32[5,1536]{1,0:T(8,128)} %slice.268) | copy-start | bytes 92164
  341.7 9.7 %copy-start.22 = (f32[1,1536]{1,0:T(1,128)S(1)}, f32[1,1536]{1,0:T(1,128)}, u32[]{:S(2)}) copy-start(f32[1,1536]{1,0:T(1,128)} %slice.284) | copy-start | bytes 18436
  344.8 6.7 copy-start.11
  344.8 6.7 copy-start.12
  351.0 2.3 copy-start.24
  351.5 2.1 copy-start.9
  351.5 2.1 copy-start.10
  353.3 0.7 copy-start.20
  353.6 1.1 copy-start.5
  353.6 1.2 copy-start.6
  354.1 0.8 copy-start.19
  365.6 2.0 copy-start.25
  367.8 5.0 copy-start.27
  372.8 27.0 %copy-start.3 = (bf16[384,1024]{1,0:T(8,128)(2,1)S(1)}, bf16[384,1024]{1,0:T(8,128)(2,1)}, u32[]{:S(2)}) copy-start(bf16[384,1024]{1,0:T(8,128)(2,1)} %param.18) | copy-start | bytes 2359300
  381.0 49.7 %all-gather.15.cloned.1.call-start = ((), (), s32[]{:S(2)}) async-start(), calls=%async_computation.6 | async-start | bytes 2359296 | tf_op jit(solution)/shard_map/all_gather | solution.py:24
  402.1 3.3 copy-start.4
  402.1 165.0 %all-gather.17.cloned.1.call-start = ((), (), s32[]{:S(2)}) async-start(), calls=%async_computation.7 | async-start | bytes 11796480 | tf_op jit(solution)/shard_map/all_gather | solution.py:123
  405.3 312.6 %all-gather.19.cloned.1.call-start = ((), (), s32[]{:S(2)}) async-start(), calls=%async_computation.8 | async-start | bytes 11796480 | tf_op jit(solution)/shard_map/all_gather | solution.py:127
  406.6 3.1 copy-start.36
  406.6 462.0 %all-gather.21.cloned.1.call-start = ((), (), s32[]{:S(2)}) async-start(), calls=%async_computation.9 | async-start | bytes 11796480 | tf_op jit(solution)/shard_map/all_gather | solution.py:136
  409.6 157.5 %copy-start.30 = (f32[2560]{0:T(1024)S(1)}, f32[2560]{0:T(1024)}, u32[]{:S(2)}) copy-start(f32[2560]{0:T(1024)} %param.31) | copy-start | bytes 30724
  409.6 157.5 %copy-start.34 = (f32[2048]{0:T(1024)S(1)}, f32[2048]{0:T(1024)}, u32[]{:S(2)}) copy-start(f32[2048]{0:T(1024)} %param.29) | copy-start | bytes 24580
  409.6 484.3 %reduce-scatter.5.cloned.1.call-start = ((), (), s32[]{:S(2)}) async-start(), calls=%async_computation.10 | async-start | bytes 2359296 | tf_op jit(solution)/shard_map/reduce_scatter | solution.py:29
  432.4 436.2 %copy-start.8 = (bf16[384,2048]{1,0:T(8,128)(2,1)S(1)}, bf16[384,2048]{1,0:T(8,128)(2,1)}, u32[]{:S(2)}) copy-start(bf16[384,2048]{1,0:T(8,128)(2,1)} %all-gather.15.cloned.1.call-done) | copy-start | bytes 4718596
  432.5 436.2 %copy-start.31 = (f32[2560]{0:T(1024)S(1)}, f32[2560]{0:T(1024)}, u32[]{:S(2)}) copy-start(f32[2560]{0:T(1024)} %param.33) | copy-start | bytes 30724
  868.6 25.2 %copy-start.2 = (bf16[384,1024]{1,0:T(8,128)(2,1)S(1)}, bf16[384,1024]{1,0:T(8,128)(2,1)}, u32[]{:S(2)}) copy-start(bf16[384,1024]{1,0:T(8,128)(2,1)} %add_convert_fusion.2) | copy-start | bytes 2359300
  868.6 27.6 %copy-start.1 = (bf16[12,128,128]{2,1,0:T(8,128)(2,1)S(1)}, bf16[12,128,128]{2,1,0:T(8,128)(2,1)}, u32[]{:S(2)}) copy-start(bf16[12,128,128]{2,1,0:T(8,128)(2,1)} %param.23) | copy-start | bytes 1179652
Sparse Core Ops, SparseCore 0:
  21.0 11.1 all-gather.10
  34.3 198.7 all-gather.12
  381.1 18.6 reduce-scatter.2
  402.2 11.0 all-gather.14
  415.4 151.6 all-gather.16
  569.1 148.6 all-gather.18
  719.9 148.6 all-gather.20
  886.7 7.1 reduce-scatter.4
